TPU v7x, 32 devices: a whole 2x2x4 slice. The times are simulated.
32 devices in a mesh: row: 8 (over z, core), col: 4 (over y, x).
Axes of the slice: x: 2, y: 2, z: 4, core: 2. Of those that a mesh axis runs over, the one named last changes fastest.
Arguments:
- mix_input: bfloat16 [4, 2048, 1024], P('col', 'row'), may hold values from -6 to 6
- gate_logits: bfloat16 [4, 2048, 2048], P('col', 'row'), may hold values from -8 to 8
- w_proj: bfloat16 [1024, 2048], P('col'), may hold values from -0.1875 to 0.1875
Outputs:
- mixed: bfloat16 [4, 2048, 2048], P('col', 'row')
All inputs are finite; a program needn't handle non-finite values.
Results may differ from a plain program's by a relative error of at most 0.0049.
Values may be sent and summed in bfloat16 or wider, within the bound.
A program may use at most 64 MiB of HBM per device.

v0:
```python
import math
import jax
import jax.numpy as jnp
from jax import lax
from jax.sharding import PartitionSpec as P

GROUP = 256
GROUPS = 4
POS_INNER = 128
highest = lax.Precision.HIGHEST


def tables(rows_in, cols_out, period):
    left_index = jnp.arange(rows_in, dtype=jnp.int32)[:, None]
    right_index = jnp.arange(cols_out, dtype=jnp.int32)[None, :]
    angles = (left_index * right_index % period).astype(jnp.float32) * (2.0 * math.pi / period)
    return (jnp.cos(angles), jnp.sin(angles))


def half_tables(group_size):
    index_row = jnp.arange(group_size, dtype=jnp.int32)
    frequency = jnp.where(index_row == 1, group_size // 2, index_row // 2)
    is_cosine = jnp.logical_or(index_row % 2 == 0, index_row == 1)
    channel = jnp.arange(group_size, dtype=jnp.int32)[:, None]
    angles = (channel * frequency[None, :] % group_size).astype(jnp.float32) * (
        2.0 * math.pi / group_size
    )
    return jnp.where(is_cosine[None, :], jnp.cos(angles), jnp.sin(angles))


def position_transform(values, inner_len):
    length, columns = values.shape
    outer_len = length // inner_len
    blocks = values.reshape(inner_len, outer_len, columns)
    cos_one, sin_one = tables(inner_len, inner_len, inner_len)
    first_re = jnp.einsum("pqc,pk->ckq", blocks, cos_one, precision=highest)
    first_im = -jnp.einsum("pqc,pk->ckq", blocks, sin_one, precision=highest)
    cos_twist, sin_twist = tables(inner_len, outer_len, length)
    second_re = first_re * cos_twist + first_im * sin_twist
    second_im = first_im * cos_twist - first_re * sin_twist
    cos_two, sin_two = tables(outer_len, outer_len, outer_len)
    whole_re = jnp.einsum("ckq,qj->cjk", second_re, cos_two, precision=highest) + jnp.einsum(
        "ckq,qj->cjk", second_im, sin_two, precision=highest
    )
    whole_im = jnp.einsum("ckq,qj->cjk", second_im, cos_two, precision=highest) - jnp.einsum(
        "ckq,qj->cjk", second_re, sin_two, precision=highest
    )
    return (whole_re.reshape(columns, length), whole_im.reshape(columns, length))


def on_device(mix_input, gate_logits, w_proj):
    tokens = mix_input[0]
    tok_count, features = tokens.shape
    row_count = lax.axis_size("row")
    length = tok_count * row_count
    norm_factor = 1.0 / math.sqrt(length * GROUP)
    grouped = tokens.astype(jnp.float32).reshape(tok_count, GROUPS, GROUP)
    packed = jnp.einsum("tgc,cm->tgm", grouped, half_tables(GROUP), precision=highest).reshape(
        tok_count, features
    )
    packed_cols = lax.all_to_all(packed, "row", split_axis=1, concat_axis=0, tiled=True)
    part_re, part_im = position_transform(packed_cols, POS_INNER)
    columns = part_re.shape[0]
    pair_re = part_re.reshape(columns // 2, 2, length)
    pair_im = part_im.reshape(columns // 2, 2, length)
    pair_index = lax.axis_index("row") * (columns // 2) + jnp.arange(columns // 2, dtype=jnp.int32)
    special = (pair_index % (GROUP // 2) == 0)[:, None]
    low_half = jnp.where(special, pair_re[:, 0], pair_re[:, 0] + pair_im[:, 1])
    high_half = jnp.where(special, pair_re[:, 1], pair_re[:, 0] - pair_im[:, 1])
    paired = (
        jnp.stack([low_half, high_half], axis=1).reshape(columns, length) * norm_factor
    ).astype(jnp.bfloat16)
    returned = lax.all_to_all(paired, "row", split_axis=1, concat_axis=0, tiled=True)
    pair_grid = returned.reshape(GROUPS, GROUP // 2, 2, tok_count)
    spectrum = jnp.concatenate(
        [pair_grid[:, :, 0], pair_grid[:, :1, 1], jnp.flip(pair_grid[:, 1:, 1], axis=1)], axis=1
    ).reshape(features, tok_count)
    projected = lax.dot_general(
        spectrum,
        lax.all_gather(w_proj, "col", axis=0, tiled=True),
        (((0,), (0,)), ((), ())),
        preferred_element_type=jnp.float32,
    )
    gate_open = jax.nn.sigmoid(gate_logits[0].astype(jnp.float32))
    return (gate_open * projected).astype(jnp.bfloat16)[None]


def solution(mesh):
    in_specs = (P("col", "row", None), P("col", "row", None), P("col", None))
    out_specs = P("col", "row", None)
    return jax.shard_map(
        on_device, mesh=mesh, in_specs=in_specs, out_specs=out_specs, check_vma=False
    )
```

profile of v0, /device:TPU:0, one launch (start us, length us, event | category | flops | bytes accessed | tf_op | source)
XLA Modules:
  0.0 91.6 jit_solution(6947621169780344983)
XLA Ops:
  6.5 0.0 all-gather.2.cloned.1.call-start
  6.5 0.7 all-gather.2.cloned.1.call-update
  7.3 1.4 %reshape.125 = bf16[256,4,256]{2,1,0:T(4,128)(2,1)S(1)} reshape(bf16[1,256,1024]{2,1,0:T(8,128)(2,1)} %param.3) | data formatting | bytes 1048576 | tf_op jit(solution)/shard_map/reshape | solution.py:57
  8.7 1.7 %fusion.8 = f32[256,256,4]{1,0,2:T(8,128)S(1)} fusion(bf16[256,4,256]{2,1,0:T(4,128)(2,1)S(1)} %reshape.125, s32[256]{0:T(256)S(1)} %fusion.67, pred[256]{0:T(512)(128)(4,1)S(1)} %compare_or_fusion), kind=kOutput, calls=%fused_computation.18 | convolution fusion | flops 806289408 | bytes 1574144 | tf_op jit(solution)/shard_map/tgc,cm->tgm/dot_general | solution.py:58
  10.4 1.3 %copy.30 = f32[256,8,128]{2,0,1:T(8,128)} copy(f32[256,8,128]{0,2,1:T(8,128)S(1)} %bitcast.61) | data formatting | bytes 2097152 | tf_op jit(solution)/shard_map/all_to_all | solution.py:61
  11.7 6.4 %all-to-all-start = ((f32[256,8,128]{2,0,1:T(8,128)}), f32[256,8,128]{2,0,1:T(8,128)S(1)}, u32[]{:S(2)}, u32[]{:S(2)}) async-start(f32[256,8,128]{2,0,1:T(8,128)} %copy.30), calls=%async_computation | async-start | bytes 2097152 | tf_op jit(solution)/shard_map/all_to_all | solution.py:61
  18.1 0.1 fusion.59
  18.2 26.5 %all-to-all-done = f32[256,8,128]{2,0,1:T(8,128)S(1)} async-done(((f32[256,8,128]{2,0,1:T(8,128)}), f32[256,8,128]{2,0,1:T(8,128)S(1)}, u32[]{:S(2)}, u32[]{:S(2)}) %all-to-all-start) | async-done | bytes 1048608 | tf_op jit(solution)/shard_map/all_to_all | solution.py:61
  44.6 1.5 %convolution_negate_fusion = f32[128,16,128]{2,0,1:T(8,128)S(1)} fusion(f32[128,16,128]{2,1,0:T(8,128)S(1)} %bitcast.56), kind=kOutput, calls=%fused_computation.7 | convolution fusion | flops 403144704 | bytes 2097152 | tf_op jit(solution)/shard_map/pqc,pk->ckq/dot_general | solution.py:37
  46.1 2.8 %subtract_bitcast_fusion = (f32[128,128,16]{0,1,2:T(8,128)S(1)}, f32[128,128,16]{0,1,2:T(8,128)}) fusion(f32[128,16,128]{2,0,1:T(8,128)S(1)} %convolution_negate_fusion, f32[128,16]{0,1:T(8,128)S(1)} %get-tuple-element.9, f32[128,16]{0,1:T(8,128)S(1)} %get-tuple-element.10, f32[128,16,128]{2,1,0:T(8,128)S(1)} %bitcast.57), kind=kOutput, calls=%fused_computation.10 | convolution fusion | flops 404455424 | bytes 4210688 | tf_op jit(solution)/shard_map/pqc,pk->ckq/dot_general | solution.py:36
  49.0 1.7 %copy.33 = f32[128,128,16]{1,2,0:T(8,128)S(1)} copy(f32[128,128,16]{0,1,2:T(8,128)} %get-tuple-element.6) | data formatting | bytes 2097152 | tf_op jit(solution)/shard_map/add | solution.py:39
  50.7 0.5 copy.34
  51.1 1.0 %fusion.51 = f32[16,128,128]{2,0,1:T(8,128)S(1)} fusion(f32[128,128,16]{1,2,0:T(8,128)S(1)} %copy.33), kind=kOutput, calls=%fused_computation.70 | convolution fusion | flops 50335232 | bytes 2097152 | tf_op jit(solution)/shard_map/ckq,qj->cjk/dot_general | solution.py:42
  52.2 1.1 %fusion.3 = f32[128,16,128]{2,1,0:T(8,128)S(1)} fusion(f32[16,128,128]{2,0,1:T(8,128)S(1)} %fusion.51, f32[128,128,16]{1,2,0:T(8,128)S(1)} %copy.34), kind=kOutput, calls=%fused_computation.6 | convolution fusion | flops 50597376 | bytes 3145728 | tf_op jit(solution)/shard_map/ckq,qj->cjk/dot_general | solution.py:42
  53.3 1.5 %reshape_reshape.6 = f32[64,2,2048]{2,1,0:T(2,128)} reshape(f32[128,16,128]{2,1,0:T(8,128)S(1)} %fusion.3) | data formatting | bytes 2097152 | tf_op jit(solution)/shard_map/reshape;reshape | solution.py:64
  54.8 1.0 %fusion.49 = f32[16,128,128]{2,0,1:T(8,128)S(1)} fusion(f32[128,128,16]{1,2,0:T(8,128)S(1)} %copy.34), kind=kOutput, calls=%fused_computation.68 | convolution fusion | flops 50335232 | bytes 2097152 | tf_op jit(solution)/shard_map/ckq,qj->cjk/dot_general | solution.py:45
  55.9 0.0 copy-start
  55.9 1.1 %fusion.2 = f32[128,16,128]{2,1,0:T(8,128)S(1)} fusion(f32[16,128,128]{2,0,1:T(8,128)S(1)} %fusion.49, f32[128,128,16]{1,2,0:T(8,128)S(1)} %copy.33), kind=kOutput, calls=%fused_computation.4 | convolution fusion | flops 50597376 | bytes 3145728 | tf_op jit(solution)/shard_map/ckq,qj->cjk/dot_general | solution.py:45
  57.0 0.5 reshape_reshape.7
  57.5 0.0 copy-done
  57.5 1.6 %broadcast_select_fusion.1 = (f32[64,1,2048]{2,1,0:T(1,128)S(1)}, f32[64,1,2048]{2,1,0:T(1,128)S(1)}) fusion(pred[64]{0:T(512)(128)(4,1)S(1)} %fusion.69, f32[64,2,2048]{2,1,0:T(2,128)S(1)} %reshape_reshape.7, f32[64,2,2048]{2,1,0:T(2,128)S(1)} %copy-done), kind=kLoop, calls=%fused_computation.13 | loop fusion | flops 524288 | bytes 2621504 | tf_op jit(solution)/shard_map/jit(_where)/select_n | solution.py:68
  59.1 1.1 %fusion.4 = bf16[64,2,2048]{2,1,0:T(2,128)(2,1)S(1)} fusion(f32[64,1,2048]{2,1,0:T(1,128)S(1)} %get-tuple-element.8, f32[64,1,2048]{2,1,0:T(1,128)S(1)} %get-tuple-element.7), kind=kLoop, calls=%fused_computation.9 | loop fusion | flops 786432 | bytes 1572864 | tf_op jit(solution)/shard_map/convert_element_type | solution.py:72
  60.2 0.3 convert_element_type.54
  60.6 0.1 copy.37
  60.7 18.0 %all_to_all.29 = bf16[128,8,256]{2,0,1:T(8,128)(2,1)S(1)} all-to-all(bf16[128,8,256]{2,0,1:T(8,128)(2,1)S(1)} %copy.37), channel_id=1, replica_groups=mesh['row'=8,'col'=4] {'row'}, dimensions={1} | all-to-all | bytes 1048576 | tf_op jit(solution)/shard_map/all_to_all | solution.py:73
  78.6 0.2 reshape.127
  78.8 0.0 copy-start.1
  78.8 0.6 slice.32
  79.5 0.5 rev.4
  80.0 0.1 pad_maximum_fusion
  80.1 0.0 all-gather.2.cloned.1.call-done
  80.1 0.0 copy-done.1
  80.1 4.6 %fusion.1 = bf16[1,256,2048]{2,1,0:T(8,128)(2,1)} fusion(bf16[1024,256]{1,0:T(8,128)(2,1)S(1)} %bitcast.63, bf16[1024,2048]{1,0:T(8,128)(2,1)} %all-gather.2.cloned.1.call-done, bf16[1,256,2048]{2,1,0:T(8,128)(2,1)S(1)} %copy-done.1), kind=kOutput, calls=%fused_computation.2 | convolution fusion | flops 1076887552 | bytes 6815744 | tf_op jit(solution)/shard_map/dot_general | solution.py:78
  (6 shorter events, 0.1 us)
Async XLA Ops:
  6.5 73.6 %all-gather.2.cloned.1.call-start = ((), (), s32[]{:S(2)}) async-start(), calls=%async_computation.2 | async-start | bytes 5242880 | tf_op jit(solution)/shard_map/all_gather | solution.py:80
  11.7 32.9 %all-to-all-start = ((f32[256,8,128]{2,0,1:T(8,128)}), f32[256,8,128]{2,0,1:T(8,128)S(1)}, u32[]{:S(2)}, u32[]{:S(2)}) async-start(f32[256,8,128]{2,0,1:T(8,128)} %copy.30), calls=%async_computation | async-start | bytes 2097152 | tf_op jit(solution)/shard_map/all_to_all | solution.py:61
  55.9 1.7 %copy-start = (f32[64,2,2048]{2,1,0:T(2,128)S(1)}, f32[64,2,2048]{2,1,0:T(2,128)}, u32[]{:S(2)}) copy-start(f32[64,2,2048]{2,1,0:T(2,128)} %reshape_reshape.6) | copy-start | bytes 3145732
  78.8 1.3 %copy-start.1 = (bf16[1,256,2048]{2,1,0:T(8,128)(2,1)S(1)}, bf16[1,256,2048]{2,1,0:T(8,128)(2,1)}, u32[]{:S(2)}) copy-start(bf16[1,256,2048]{2,1,0:T(8,128)(2,1)} %param.4) | copy-start | bytes 3145732
Sparse Core Ops, SparseCore 0:
  9.2 55.2 all-gather.1
where the time goes:
time: 91.9 us; the launch traced here: 91.6 us
  waiting for transfers between devices  27.2 us (30%)
  blocking collectives  18 us (20%)
  matrix products  14.9 us (16%)
  between operations  13.6 us (15%)
  local copies, waits for them, and re-layouts  8.74 us (10%)
  starting transfers between devices  6.36 us (7%)
  other arithmetic  2.85 us (3%)
    all_to_all x1, waiting for transfers between devices, on_device(): lax.all_to_all(packed, 'row', split_axis=1, concat_axis=0, tiled=True)  26.5 us
    all_to_all x1, blocking collectives, on_device(): lax.all_to_all(paired, 'row', split_axis=1, concat_axis=0, tiled=True)  18 us
    all_to_all x1, starting transfers between devices, on_device(): lax.all_to_all(packed, 'row', split_axis=1, concat_axis=0, tiled=True)  6.35 us
    dot_general x1, matrix products, on_device(): lax.dot_general(spectrum, lax.all_gather(w_proj, 'col', axis=0, tiled=Tru...  4.64 us
    dot_general x1, matrix products, position_transform(): first_re = jnp.einsum('pqc,pk->ckq', blocks, cos_one, precision=highest)  2.84 us
  transfers between devices with their start and end apart: 2, of which 1 were waited for; matrix products, arithmetic and copies ran while one was open for 24% of the time, Pallas kernels for 0%

commit v1 on v0

--- a/solution.py
+++ b/solution.py
@@ -8,6 +8,17 @@
 GROUPS = 4
 POS_INNER = 128
 highest = lax.Precision.HIGHEST
+
+
+def split_up(array, dim, size):
+    before, after = (array.shape[:dim], array.shape[dim + 1 :])
+    return jnp.moveaxis(array.reshape(*before, size, -1, *after), dim, 0)
+
+
+def joined_along(parts, dim):
+    parts = jnp.moveaxis(parts, 0, dim)
+    dims = parts.shape
+    return parts.reshape(*dims[:dim], dims[dim] * dims[dim + 1], *dims[dim + 2 :])
 
 
 def tables(rows_in, cols_out, period):
@@ -58,7 +69,14 @@
     packed = jnp.einsum("tgc,cm->tgm", grouped, half_tables(GROUP), precision=highest).reshape(
         tok_count, features
     )
-    packed_cols = lax.all_to_all(packed, "row", split_axis=1, concat_axis=0, tiled=True)
+    count, mine = (lax.axis_size("row"), lax.axis_index("row"))
+    tiles = split_up(packed, 1, count)
+    outs = [tiles[mine]]
+    for step in range(1, count):
+        sent = tiles[(mine + step) % count]
+        outs.append(lax.ppermute(sent, "row", [(i, (i + step) % count) for i in range(count)]))
+    tiles = jnp.stack(outs)[(mine - jnp.arange(count)) % count]
+    packed_cols = joined_along(tiles, 0)
     part_re, part_im = position_transform(packed_cols, POS_INNER)
     columns = part_re.shape[0]
     pair_re = part_re.reshape(columns // 2, 2, length)

time: 91.9 us -> 87.1 us (0.948)
  waiting for transfers between devices: 27.2 us -> 8.73 us
  blocking collectives: 18 us -> 25.8 us
  starting transfers between devices: 6.36 us -> 11.6 us
    all_to_all x1 -> x0, waiting for transfers between devices: 26.5 us -> none  [on_device(): lax.all_to_all(packed, 'row', split_axis=1, concat_axis=0, tiled=True)]
    ppermute x0 -> x7, starting transfers between devices: none -> 11.6 us  [on_device(): lax.ppermute(sent, 'row', [(i, (i + step) % count) for i in range(count)])]
    ppermute x0 -> x7, waiting for transfers between devices: none -> 8 us  [on_device(): lax.ppermute(sent, 'row', [(i, (i + step) % count) for i in range(count)])]
    all_to_all x1, blocking collectives: 18 us -> 25.8 us  [on_device(): lax.all_to_all(paired, 'row', split_axis=1, concat_axis=0, tiled=True)]
    all_to_all x1 -> x0, starting transfers between devices: 6.35 us -> none  [on_device(): lax.all_to_all(packed, 'row', split_axis=1, concat_axis=0, tiled=True)]
    all_to_all x1 -> x0, local copies, waits for them, and re-layouts: 1.31 us -> none  [on_device(): lax.all_to_all(packed, 'row', split_axis=1, concat_axis=0, tiled=True)]
  transfers between devices with their start and end apart: 2 -> 8, of which waited for: 1 -> 3; matrix products, arithmetic and copies ran while one was open for 24% -> 26% of each run, Pallas kernels for 0% -> 0%
where the time goes in v1:
time: 87.1 us; the launch traced here: 86.9 us
  blocking collectives  25.8 us (30%)
  matrix products  14.8 us (17%)
  between operations  13.9 us (16%)
  starting transfers between devices  11.6 us (13%)
  local copies, waits for them, and re-layouts  8.98 us (10%)
  waiting for transfers between devices  8.73 us (10%)
  other arithmetic  3.1 us (4%)
    all_to_all x1, blocking collectives, on_device(): lax.all_to_all(paired, 'row', split_axis=1, concat_axis=0, tiled=True)  25.8 us
    ppermute x7, starting transfers between devices, on_device(): lax.ppermute(sent, 'row', [(i, (i + step) % count) for i in range(count)])  11.6 us
    ppermute x7, waiting for transfers between devices, on_device(): lax.ppermute(sent, 'row', [(i, (i + step) % count) for i in range(count)])  8 us
    dot_general x1, matrix products, on_device(): lax.dot_general(spectrum, lax.all_gather(w_proj, 'col', axis=0, tiled=Tru...  4.64 us
    dot_general x1, matrix products, position_transform(): first_re = jnp.einsum('pqc,pk->ckq', blocks, cos_one, precision=highest)  2.79 us
    select_n x1, other arithmetic, on_device(): low_half = jnp.where(special, pair_re[:, 0], pair_re[:, 0] + pair_im[:, 1])  1.78 us
  transfers between devices with their start and end apart: 8, of which 3 were waited for; matrix products, arithmetic and copies ran while one was open for 26% of the time, Pallas kernels for 0%

profile of v1, /device:TPU:0, one launch (start us, length us, event | category | flops | bytes accessed | tf_op | source)
XLA Modules:
  0.0 86.9 jit_solution(7564460208654972078)
XLA Ops:
  6.5 0.7 all-gather.2.cloned.1.call-update
  7.3 1.4 %reshape.180 = bf16[256,4,256]{2,1,0:T(4,128)(2,1)S(1)} reshape(bf16[1,256,1024]{2,1,0:T(8,128)(2,1)} %param.3) | data formatting | bytes 1048576 | tf_op jit(solution)/shard_map/reshape | solution.py:68
  8.7 1.7 %fusion.8 = f32[256,256,4]{1,0,2:T(8,128)S(1)} fusion(bf16[256,4,256]{2,1,0:T(4,128)(2,1)S(1)} %reshape.180, s32[256]{0:T(256)S(1)} %fusion.74, pred[256]{0:T(512)(128)(4,1)S(1)} %compare_or_fusion), kind=kOutput, calls=%fused_computation.19 | convolution fusion | flops 806289408 | bytes 1574144 | tf_op jit(solution)/shard_map/tgc,cm->tgm/dot_general | solution.py:69
  10.5 0.1 constant_dynamic-slice_fusion
  10.6 0.1 copy.37
  10.7 0.5 collective-permute-start
  11.3 0.1 copy.38
  11.3 2.6 %collective-permute-start.1 = (f32[256,128]{1,0:T(8,128)S(1)}, f32[256,128]{1,0:T(8,128)S(1)}, u32[]{:S(2)}, u32[]{:S(2)}) collective-permute-start(f32[256,128]{1,0:T(8,128)S(1)} %bitcast.90), channel_id=1, source_target_pairs={{0,8},{4,12},{8,16},{12,20},{16,24},{20,28},{24,0},{28,4},{1,9},{5... | collective-permute-start | bytes 393224 | tf_op jit(solution)/shard_map/ppermute | solution.py:77
  14.0 0.1 copy.39
  14.1 2.6 %collective-permute-start.2 = (f32[256,128]{1,0:T(8,128)S(1)}, f32[256,128]{1,0:T(8,128)S(1)}, u32[]{:S(2)}, u32[]{:S(2)}) collective-permute-start(f32[256,128]{1,0:T(8,128)S(1)} %bitcast.89), channel_id=1, source_target_pairs={{0,12},{4,16},{8,20},{12,24},{16,28},{20,0},{24,4},{28,8},{1,13},{... | collective-permute-start | bytes 393224 | tf_op jit(solution)/shard_map/ppermute | solution.py:77
  16.7 0.1 copy.40
  16.8 1.3 %collective-permute-start.3 = (f32[256,128]{1,0:T(8,128)S(1)}, f32[256,128]{1,0:T(8,128)S(1)}, u32[]{:S(2)}, u32[]{:S(2)}) collective-permute-start(f32[256,128]{1,0:T(8,128)S(1)} %bitcast.88), channel_id=1, source_target_pairs={{0,16},{4,20},{8,24},{12,28},{16,0},{20,4},{24,8},{28,12},{1,17},{... | collective-permute-start | bytes 393224 | tf_op jit(solution)/shard_map/ppermute | solution.py:77
  18.1 0.1 copy.41
  18.2 1.2 %collective-permute-start.4 = (f32[256,128]{1,0:T(8,128)S(1)}, f32[256,128]{1,0:T(8,128)S(1)}, u32[]{:S(2)}, u32[]{:S(2)}) collective-permute-start(f32[256,128]{1,0:T(8,128)S(1)} %bitcast.87), channel_id=1, source_target_pairs={{0,20},{4,24},{8,28},{12,0},{16,4},{20,8},{24,12},{28,16},{1,21},{... | collective-permute-start | bytes 393224 | tf_op jit(solution)/shard_map/ppermute | solution.py:77
  19.4 0.1 copy.36
  19.5 0.1 copy.42
  19.6 0.1 copy.43
  19.7 0.1 fusion.59
  19.8 0.0 collective-permute-done
  19.8 1.4 %collective-permute-start.5 = (f32[256,128]{1,0:T(8,128)S(1)}, f32[256,128]{1,0:T(8,128)S(1)}, u32[]{:S(2)}, u32[]{:S(2)}) collective-permute-start(f32[256,128]{1,0:T(8,128)S(1)} %bitcast.92), channel_id=1, source_target_pairs={{0,24},{4,28},{8,0},{12,4},{16,8},{20,12},{24,16},{28,20},{1,25},{... | collective-permute-start | bytes 393224 | tf_op jit(solution)/shard_map/ppermute | solution.py:77
  21.3 1.9 %collective-permute-start.6 = (f32[256,128]{1,0:T(8,128)S(1)}, f32[256,128]{1,0:T(8,128)S(1)}, u32[]{:S(2)}, u32[]{:S(2)}) collective-permute-start(f32[256,128]{1,0:T(8,128)S(1)} %bitcast.91), channel_id=1, source_target_pairs={{0,28},{4,0},{8,4},{12,8},{16,12},{20,16},{24,20},{28,24},{1,29},{... | collective-permute-start | bytes 393224 | tf_op jit(solution)/shard_map/ppermute | solution.py:77
  23.1 7.4 %collective-permute-done.2 = f32[256,128]{1,0:T(8,128)S(1)} collective-permute-done((f32[256,128]{1,0:T(8,128)S(1)}, f32[256,128]{1,0:T(8,128)S(1)}, u32[]{:S(2)}, u32[]{:S(2)}) %collective-permute-start.2) | collective-permute-done | bytes 131104 | tf_op jit(solution)/shard_map/ppermute | solution.py:77
  30.5 0.2 collective-permute-done.3
  30.8 0.4 collective-permute-done.6
  31.2 0.6 gather_fusion
  31.9 1.5 %convolution_negate_fusion = f32[128,16,128]{2,0,1:T(8,128)S(1)} fusion(f32[128,16,128]{2,1,0:T(8,128)S(1)} %bitcast.79), kind=kOutput, calls=%fused_computation.8 | convolution fusion | flops 403144704 | bytes 2097152 | tf_op jit(solution)/shard_map/pqc,pk->ckq/dot_general | solution.py:48
  33.3 2.8 %subtract_bitcast_fusion = (f32[128,128,16]{0,1,2:T(8,128)S(1)}, f32[128,128,16]{0,1,2:T(8,128)}) fusion(f32[128,16,128]{2,0,1:T(8,128)S(1)} %convolution_negate_fusion, f32[128,16]{0,1:T(8,128)S(1)} %get-tuple-element.17, f32[128,16]{0,1:T(8,128)S(1)} %get-tuple-element.18, f32[128,16,128]{2,1,0:T(8,128)S(1)} %bitcast.80), kind=kOutput, calls=%fused_computation.11 | convolution fusion | flops 404455424 | bytes 4210688 | tf_op jit(solution)/shard_map/pqc,pk->ckq/dot_general | solution.py:47
  36.1 1.7 %copy.46 = f32[128,128,16]{1,2,0:T(8,128)S(1)} copy(f32[128,128,16]{0,1,2:T(8,128)} %get-tuple-element.6) | data formatting | bytes 2097152 | tf_op jit(solution)/shard_map/add | solution.py:50
  37.8 0.5 copy.47
  38.4 1.0 %fusion.51 = f32[16,128,128]{2,0,1:T(8,128)S(1)} fusion(f32[128,128,16]{1,2,0:T(8,128)S(1)} %copy.46), kind=kOutput, calls=%fused_computation.79 | convolution fusion | flops 50335232 | bytes 2097152 | tf_op jit(solution)/shard_map/ckq,qj->cjk/dot_general | solution.py:53
  39.4 1.0 %fusion.3 = f32[128,16,128]{2,1,0:T(8,128)S(1)} fusion(f32[16,128,128]{2,0,1:T(8,128)S(1)} %fusion.51, f32[128,128,16]{1,2,0:T(8,128)S(1)} %copy.47), kind=kOutput, calls=%fused_computation.7 | convolution fusion | flops 50597376 | bytes 3145728 | tf_op jit(solution)/shard_map/ckq,qj->cjk/dot_general | solution.py:53
  40.5 1.5 %reshape_reshape.14 = f32[64,2,2048]{2,1,0:T(2,128)} reshape(f32[128,16,128]{2,1,0:T(8,128)S(1)} %fusion.3) | data formatting | bytes 2097152 | tf_op jit(solution)/shard_map/reshape;reshape | solution.py:82
  42.0 1.0 %fusion.49 = f32[16,128,128]{2,0,1:T(8,128)S(1)} fusion(f32[128,128,16]{1,2,0:T(8,128)S(1)} %copy.47), kind=kOutput, calls=%fused_computation.77 | convolution fusion | flops 50335232 | bytes 2097152 | tf_op jit(solution)/shard_map/ckq,qj->cjk/dot_general | solution.py:56
  43.0 0.0 copy-start
  43.0 1.0 %fusion.2 = f32[128,16,128]{2,1,0:T(8,128)S(1)} fusion(f32[16,128,128]{2,0,1:T(8,128)S(1)} %fusion.49, f32[128,128,16]{1,2,0:T(8,128)S(1)} %copy.46), kind=kOutput, calls=%fused_computation.5 | convolution fusion | flops 50597376 | bytes 3145728 | tf_op jit(solution)/shard_map/ckq,qj->cjk/dot_general | solution.py:56
  44.1 0.5 reshape_reshape.15
  44.6 1.8 %broadcast_select_fusion.1 = (f32[64,1,2048]{2,1,0:T(1,128)S(1)}, f32[64,1,2048]{2,1,0:T(1,128)S(1)}) fusion(pred[64]{0:T(512)(128)(4,1)S(1)} %fusion.76, f32[64,2,2048]{2,1,0:T(2,128)S(1)} %reshape_reshape.15, f32[64,2,2048]{2,1,0:T(2,128)S(1)} %copy-done), kind=kLoop, calls=%fused_computation.14 | loop fusion | flops 524288 | bytes 2621504 | tf_op jit(solution)/shard_map/jit(_where)/select_n | solution.py:86
  46.4 1.1 %fusion.4 = bf16[64,2,2048]{2,1,0:T(2,128)(2,1)S(1)} fusion(f32[64,1,2048]{2,1,0:T(1,128)S(1)} %get-tuple-element.8, f32[64,1,2048]{2,1,0:T(1,128)S(1)} %get-tuple-element.7), kind=kLoop, calls=%fused_computation.10 | loop fusion | flops 786432 | bytes 1572864 | tf_op jit(solution)/shard_map/convert_element_type | solution.py:90
  47.6 0.3 convert_element_type.54
  47.9 0.1 copy.50
  48.0 25.8 %all_to_all.13 = bf16[128,8,256]{2,0,1:T(8,128)(2,1)S(1)} all-to-all(bf16[128,8,256]{2,0,1:T(8,128)(2,1)S(1)} %copy.50), channel_id=1, replica_groups=mesh['row'=8,'col'=4] {'row'}, dimensions={1} | all-to-all | bytes 1048576 | tf_op jit(solution)/shard_map/all_to_all | solution.py:91
  73.9 0.2 reshape.181
  74.1 0.0 copy-start.1
  74.1 0.6 slice.34
  74.7 0.5 rev.4
  75.2 0.1 pad_maximum_fusion
  75.3 0.0 all-gather.2.cloned.1.call-done
  75.4 4.6 %fusion.1 = bf16[1,256,2048]{2,1,0:T(8,128)(2,1)} fusion(bf16[1024,256]{1,0:T(8,128)(2,1)S(1)} %bitcast.86, bf16[1024,2048]{1,0:T(8,128)(2,1)} %all-gather.2.cloned.1.call-done, bf16[1,256,2048]{2,1,0:T(8,128)(2,1)S(1)} %copy-done.1), kind=kOutput, calls=%fused_computation.3 | convolution fusion | flops 1076887552 | bytes 6815744 | tf_op jit(solution)/shard_map/dot_general | solution.py:96
  (22 shorter events, 0.2 us)
Async XLA Ops:
  6.5 68.8 %all-gather.2.cloned.1.call-start = ((), (), s32[]{:S(2)}) async-start(), calls=%async_computation.1 | async-start | bytes 5242880 | tf_op jit(solution)/shard_map/all_gather | solution.py:98
  10.7 9.1 %collective-permute-start = (f32[256,128]{1,0:T(8,128)S(1)}, f32[256,128]{1,0:T(8,128)S(1)}, u32[]{:S(2)}, u32[]{:S(2)}) collective-permute-start(f32[256,128]{1,0:T(8,128)S(1)} %bitcast.93), channel_id=1, source_target_pairs={{0,4},{4,8},{8,12},{12,16},{16,20},{20,24},{24,28},{28,0},{1,5},{5... | collective-permute-start | bytes 393224 | tf_op jit(solution)/shard_map/ppermute | solution.py:77
  11.3 9.9 %collective-permute-start.1 = (f32[256,128]{1,0:T(8,128)S(1)}, f32[256,128]{1,0:T(8,128)S(1)}, u32[]{:S(2)}, u32[]{:S(2)}) collective-permute-start(f32[256,128]{1,0:T(8,128)S(1)} %bitcast.90), channel_id=1, source_target_pairs={{0,8},{4,12},{8,16},{12,20},{16,24},{20,28},{24,0},{28,4},{1,9},{5... | collective-permute-start | bytes 393224 | tf_op jit(solution)/shard_map/ppermute | solution.py:77
  14.1 16.4 %collective-permute-start.2 = (f32[256,128]{1,0:T(8,128)S(1)}, f32[256,128]{1,0:T(8,128)S(1)}, u32[]{:S(2)}, u32[]{:S(2)}) collective-permute-start(f32[256,128]{1,0:T(8,128)S(1)} %bitcast.89), channel_id=1, source_target_pairs={{0,12},{4,16},{8,20},{12,24},{16,28},{20,0},{24,4},{28,8},{1,13},{... | collective-permute-start | bytes 393224 | tf_op jit(solution)/shard_map/ppermute | solution.py:77
  16.8 13.9 %collective-permute-start.3 = (f32[256,128]{1,0:T(8,128)S(1)}, f32[256,128]{1,0:T(8,128)S(1)}, u32[]{:S(2)}, u32[]{:S(2)}) collective-permute-start(f32[256,128]{1,0:T(8,128)S(1)} %bitcast.88), channel_id=1, source_target_pairs={{0,16},{4,20},{8,24},{12,28},{16,0},{20,4},{24,8},{28,12},{1,17},{... | collective-permute-start | bytes 393224 | tf_op jit(solution)/shard_map/ppermute | solution.py:77
  18.2 12.5 %collective-permute-start.4 = (f32[256,128]{1,0:T(8,128)S(1)}, f32[256,128]{1,0:T(8,128)S(1)}, u32[]{:S(2)}, u32[]{:S(2)}) collective-permute-start(f32[256,128]{1,0:T(8,128)S(1)} %bitcast.87), channel_id=1, source_target_pairs={{0,20},{4,24},{8,28},{12,0},{16,4},{20,8},{24,12},{28,16},{1,21},{... | collective-permute-start | bytes 393224 | tf_op jit(solution)/shard_map/ppermute | solution.py:77
  19.8 10.9 %collective-permute-start.5 = (f32[256,128]{1,0:T(8,128)S(1)}, f32[256,128]{1,0:T(8,128)S(1)}, u32[]{:S(2)}, u32[]{:S(2)}) collective-permute-start(f32[256,128]{1,0:T(8,128)S(1)} %bitcast.92), channel_id=1, source_target_pairs={{0,24},{4,28},{8,0},{12,4},{16,8},{20,12},{24,16},{28,20},{1,25},{... | collective-permute-start | bytes 393224 | tf_op jit(solution)/shard_map/ppermute | solution.py:77
  21.3 10.0 %collective-permute-start.6 = (f32[256,128]{1,0:T(8,128)S(1)}, f32[256,128]{1,0:T(8,128)S(1)}, u32[]{:S(2)}, u32[]{:S(2)}) collective-permute-start(f32[256,128]{1,0:T(8,128)S(1)} %bitcast.91), channel_id=1, source_target_pairs={{0,28},{4,0},{8,4},{12,8},{16,12},{20,16},{24,20},{28,24},{1,29},{... | collective-permute-start | bytes 393224 | tf_op jit(solution)/shard_map/ppermute | solution.py:77
  43.0 1.6 %copy-start = (f32[64,2,2048]{2,1,0:T(2,128)S(1)}, f32[64,2,2048]{2,1,0:T(2,128)}, u32[]{:S(2)}) copy-start(f32[64,2,2048]{2,1,0:T(2,128)} %reshape_reshape.14) | copy-start | bytes 3145732
  74.1 1.3 %copy-start.1 = (bf16[1,256,2048]{2,1,0:T(8,128)(2,1)S(1)}, bf16[1,256,2048]{2,1,0:T(8,128)(2,1)}, u32[]{:S(2)}) copy-start(bf16[1,256,2048]{2,1,0:T(8,128)(2,1)} %param.4) | copy-start | bytes 3145732
Sparse Core Ops, SparseCore 0:
  9.2 55.2 all-gather.1
